TPU v7x, 32 devices: a whole 2x2x4 slice. The times are simulated.
32 devices in a mesh: kv: 8 (over z, y), tp: 4 (over x, core).
Axes of the slice: x: 2, y: 2, z: 4, core: 2. Of those that a mesh axis runs over, the one named last changes fastest.
Arguments:
- residual: bfloat16 [256, 2048], P('kv', 'tp'), may hold values from -12 to 12
- first_gain: bfloat16 [2048], P('tp'), may hold values from 0.099609375 to 1.8984375
- first_gate: bfloat16 [2048, 5632], P('tp', 'kv'), may hold values from -0.125 to 0.125
- first_lift: bfloat16 [2048, 5632], P('tp', 'kv'), may hold values from -0.125 to 0.125
- first_down: bfloat16 [5632, 2048], P('kv', 'tp'), may hold values from -0.078125 to 0.078125
- mixer_gain: bfloat16 [2048], replicated, may hold values from 0.099609375 to 1.8984375
- proj_gate: bfloat16 [2048, 2048], P(None, 'tp'), may hold values from -0.125 to 0.125
- proj_input: bfloat16 [2048, 2048], P(None, 'tp'), may hold values from -0.125 to 0.125
- proj_write: bfloat16 [2048, 1024], P(None, 'tp'), may hold values from -0.125 to 0.125
- proj_read: bfloat16 [2048, 1024], P(None, 'tp'), may hold values from -0.125 to 0.125
- proj_step: bfloat16 [2048, 32], P(None, 'tp'), may hold values from -0.125 to 0.125
- step_bias: float32 [32], P('tp'), may hold values from -5 to -2
- rate_log: float32 [32], P('tp'), may hold values from -0.7 to 2.1
- skip_gain: float32 [32], P('tp'), may hold values from 0.5 to 2
- taps_input: bfloat16 [4, 2048], P(None, 'tp'), may hold values from -3 to 3
- taps_write: bfloat16 [4, 1024], P(None, 'tp'), may hold values from -3 to 3
- taps_read: bfloat16 [4, 1024], P(None, 'tp'), may hold values from -3 to 3
- buffer_input: bfloat16 [256, 3, 2048], P('kv', None, 'tp'), may hold values from -6 to 6
- buffer_write: bfloat16 [256, 3, 1024], P('kv', None, 'tp'), may hold values from -6 to 6
- buffer_read: bfloat16 [256, 3, 1024], P('kv', None, 'tp'), may hold values from -6 to 6
- scan_state: float32 [256, 32, 64, 128], P('kv', 'tp'), may hold values from -1.5 to 1.5
- group_gain: bfloat16 [2048], P('tp'), may hold values from 0.099609375 to 1.8984375
- proj_output: bfloat16 [2048, 2048], P('tp'), may hold values from -0.125 to 0.125
- second_gain: bfloat16 [2048], P('tp'), may hold values from 0.099609375 to 1.8984375
- second_gate: bfloat16 [2048, 5632], P('tp', 'kv'), may hold values from -0.125 to 0.125
- second_lift: bfloat16 [2048, 5632], P('tp', 'kv'), may hold values from -0.125 to 0.125
- second_down: bfloat16 [5632, 2048], P('kv', 'tp'), may hold values from -0.078125 to 0.078125
Outputs:
- residual_out: bfloat16 [256, 2048], P('kv', 'tp')
- state_out: float32 [256, 32, 64, 128], P('kv', 'tp')
All inputs are finite; a program needn't handle non-finite values.
Results may differ from a plain program's by a relative error of at most 0.023.
Values may be sent and summed in bfloat16 or wider, within the bound.
A program may use at most 64 MiB of HBM per device.

v0:
```python
import functools

import jax
import jax.numpy as jnp
from jax import lax
from jax.experimental import pallas as pl
from jax.experimental.pallas import tpu as pltpu
from jax.sharding import PartitionSpec as P

HEAD_DIM = 64
STATE = 128
EPS = 1e-06
MESH = pl.DeviceIdType.MESH
F32 = jnp.float32
BF16 = jnp.bfloat16
VMEM_LIMIT = 60 * 1024 * 1024


def silu(v):
    return v / (1.0 + jnp.exp(-v))


def dot(a, b):
    return jnp.dot(a, b, preferred_element_type=F32)


def dot_t(a, b):
    return lax.dot_general(a, b, (((1,), (1,)), ((), ())), preferred_element_type=F32)


def enter(nk, nt, kv, tp):
    barrier = pltpu.get_barrier_semaphore()
    for d in range(1, nk):
        pl.semaphore_signal(
            barrier, inc=1, device_id={"kv": lax.rem(kv + d, nk)}, device_id_type=MESH
        )
    for d in range(1, nt):
        pl.semaphore_signal(
            barrier, inc=1, device_id={"tp": lax.rem(tp + d, nt)}, device_id_type=MESH
        )
    pl.semaphore_wait(barrier, nk + nt - 2)


def far_first(n):
    return sorted(range(1, n), key=lambda d: -min(d, n - d))


def remote(src, dst, send, recv, where):
    return pltpu.make_async_remote_copy(
        src_ref=src, dst_ref=dst, send_sem=send, recv_sem=recv,
        device_id=where, device_id_type=MESH,
    )


def half_scratch(nk, nt, rows, width, cols):
    total = nk * rows
    share = total // nt
    dma = pltpu.SemaphoreType.DMA
    return [
        pltpu.VMEM((cols, width), BF16),
        pltpu.VMEM((cols, width), BF16),
        pltpu.VMEM((cols, width), BF16),
        dma((3,)),
        pltpu.VMEM((total, width), BF16),
        pltpu.VMEM((total, width), BF16),
        pltpu.VMEM((total, 128), F32),
        pltpu.VMEM((nt, share, 128), F32),
        pltpu.VMEM((nt, 2, share, cols), BF16),
        pltpu.VMEM((nt, 2, share, cols), BF16),
        pltpu.VMEM((total, cols), BF16),
        pltpu.VMEM((total, width), BF16),
        pltpu.VMEM((nk, rows, width), BF16),
        dma((nk,)), dma((nk,)),
        dma((nt,)), dma((nt,)),
        dma((nt,)), dma((nt,)),
        dma((nt,)), dma((nt,)),
        dma((nk,)), dma((nk,)),
    ]


def start_weights(gate_hbm, lift_hbm, down_hbm, scratch):
    wg, wu, wd, wsem = scratch[:4]
    copies = [
        pltpu.make_async_copy(gate_hbm, wg, wsem.at[0]),
        pltpu.make_async_copy(lift_hbm, wu, wsem.at[1]),
        pltpu.make_async_copy(down_hbm, wd, wsem.at[2]),
    ]
    for c in copies:
        c.start()
    return copies


def half_body(nk, nt, kv, tp, place, x_ref, gain_ref, weights, scratch):
    (wg, wu, wd, _, xall, xg, ssq, ssr, part, parr, hid, dpart, dparr,
     ag_s, ag_r, sq_s, sq_r, rs_s, rs_r, hg_s, hg_r, dn_s, dn_r) = scratch
    rows, width = x_ref.shape
    total = nk * rows
    share = total // nt
    per = share // rows
    features = width * nt
    sends = []
    gathers = []
    for d in far_first(nk):
        c = remote(x_ref, xall.at[pl.ds(kv * rows, rows)], ag_s.at[d], ag_r.at[d],
                   {"kv": lax.rem(kv + d, nk)})
        c.start()
        gathers.append(c)
    xall[pl.ds(kv * rows, rows), :] = x_ref[...]
    gain = gain_ref[:, place * width:(place + 1) * width].astype(F32)
    for c in reversed(gathers):
        c.wait_recv()
    for k in range(nk):
        at = pl.ds(k * rows, rows)
        value = xall[at, :].astype(F32)
        ssq[at, :] = jnp.broadcast_to(
            jnp.sum(value * value, axis=1, keepdims=True), (rows, 128)
        )
        xg[at, :] = (value * gain).astype(BF16)
    squares = []
    for d in far_first(nt):
        to = lax.rem(tp + d, nt)
        c = remote(ssq.at[pl.ds(to * share, share)], ssr.at[d], sq_s.at[d], sq_r.at[d],
                   {"tp": to})
        c.start()
        squares.append(c)
    weights[0].wait()
    weights[1].wait()
    parts = []
    for d in far_first(nt) + [0]:
        to = lax.rem(tp + d, nt)
        a = xg[pl.ds(to * share, share), :]
        part[d, 0] = dot_t(a, wg[...]).astype(BF16)
        part[d, 1] = dot_t(a, wu[...]).astype(BF16)
        if d:
            c = remote(part.at[d], parr.at[d], rs_s.at[d], rs_r.at[d], {"tp": to})
            c.start()
            parts.append(c)
    mine = pl.ds(tp * share, share)
    sq = ssq[mine, :]
    for d, c in zip(far_first(nt), squares):
        c.wait_recv()
        sq = sq + ssr[d]
    factor = lax.rsqrt(sq[:, :1] / features + EPS)
    gate = part[0, 0].astype(F32)
    lift = part[0, 1].astype(F32)
    for d, c in reversed(list(zip(far_first(nt), parts))):
        c.wait_recv()
        gate = gate + parr[d, 0].astype(F32)
        lift = lift + parr[d, 1].astype(F32)
    gate = gate * factor
    lift = lift * factor
    hid[mine, :] = (silu(gate) * lift).astype(BF16)
    spread = {}
    for d in far_first(nt):
        c = remote(hid.at[mine], hid.at[mine], hg_s.at[d], hg_r.at[d],
                   {"tp": lax.rem(tp + d, nt)})
        c.start()
        spread[d] = c
    weights[2].wait()
    for d in [0] + list(reversed(far_first(nt))):
        if d:
            spread[d].wait_recv()
        source = lax.rem(tp + nt - d, nt)
        block = pl.ds(source * share, share)
        dpart[block, :] = dot(hid[block, :], wd[...]).astype(BF16)
        for j in range(per):
            to = source * per + j

            @pl.when(to != kv)
            def _():
                remote(dpart.at[pl.ds(to * rows, rows)], dparr.at[kv], dn_s.at[to],
                       dn_r.at[kv], {"kv": to}).start()

    acc = dpart[pl.ds(kv * rows, rows), :].astype(F32)
    for d in reversed(far_first(nk)):
        source = lax.rem(kv + nk - d, nk)
        pltpu.make_async_copy(dparr.at[source], dparr.at[source], dn_r.at[source]).wait()
        acc = acc + dparr[source].astype(F32)
    for d in far_first(nk):
        to = lax.rem(kv + d, nk)
        pltpu.make_async_copy(dparr.at[to], dparr.at[to], dn_s.at[to]).wait()
    for c in gathers + squares + parts + list(spread.values()):
        c.wait_send()
    return (x_ref[...].astype(F32) + 0.5 * acc).astype(BF16)


def first_kernel(nk, nt, x_ref, gain_ref, gate, lift, down, own_ref, all_ref, *scratch):
    kv, tp = lax.axis_index("kv"), lax.axis_index("tp")
    held, f_s, f_r = scratch[:3]
    scratch = scratch[3:]
    weights = start_weights(gate, lift, down, scratch)
    enter(nk, nt, kv, tp)
    out = half_body(nk, nt, kv, tp, 0, x_ref, gain_ref, weights, scratch)
    own_ref[...] = out
    held[tp] = out
    copies = []
    for d in far_first(nt):
        c = remote(held.at[tp], held.at[tp], f_s.at[d], f_r.at[d],
                   {"tp": lax.rem(tp + d, nt)})
        c.start()
        copies.append(c)
    for c in copies:
        c.wait_recv()
    all_ref[...] = held[...]
    for c in copies:
        c.wait_send()


def second_kernel(nk, nt, own_ref, pout_ref, gain_ref, gate, lift, down, out_ref, *scratch):
    kv, tp = lax.axis_index("kv"), lax.axis_index("tp")
    arrived, x_buf, m_s, m_r = scratch[:4]
    scratch = scratch[4:]
    weights = start_weights(gate, lift, down, scratch)
    enter(nk, nt, kv, tp)
    copies = []
    for d in far_first(nt):
        to = lax.rem(tp + d, nt)
        c = remote(pout_ref.at[to], arrived.at[d], m_s.at[d], m_r.at[d], {"tp": to})
        c.start()
        copies.append(c)
    acc = own_ref[...].astype(F32) + pout_ref[tp].astype(F32)
    for d, c in zip(far_first(nt), copies):
        c.wait_recv()
        acc = acc + arrived[d].astype(F32)
    x_buf[...] = acc.astype(BF16)
    out_ref[...] = half_body(nk, nt, kv, tp, 1, x_buf, gain_ref, weights, scratch)
    for c in copies:
        c.wait_send()


def vmem(n):
    return [pl.BlockSpec(memory_space=pltpu.VMEM)] * n


def params(cid):
    return pltpu.CompilerParams(
        collective_id=cid, has_side_effects=True, vmem_limit_bytes=VMEM_LIMIT
    )


def first_half(nk, nt, x, gain, gate, lift, down):
    rows, width = x.shape
    dma = pltpu.SemaphoreType.DMA
    return pl.pallas_call(
        functools.partial(first_kernel, nk, nt),
        out_shape=(jax.ShapeDtypeStruct(x.shape, BF16),
                   jax.ShapeDtypeStruct((nt, rows, width), BF16)),
        in_specs=vmem(2) + [pl.BlockSpec(memory_space=pl.ANY)] * 3,
        out_specs=tuple(vmem(2)),
        scratch_shapes=[pltpu.VMEM((nt, rows, width), BF16), dma((nt,)), dma((nt,))]
        + half_scratch(nk, nt, rows, width, gate.shape[0]),
        compiler_params=params(1),
        name="first_half",
    )(x, gain, gate, lift, down)


def second_half(nk, nt, own, pout, gain, gate, lift, down):
    rows, width = own.shape
    dma = pltpu.SemaphoreType.DMA
    return pl.pallas_call(
        functools.partial(second_kernel, nk, nt),
        out_shape=jax.ShapeDtypeStruct(own.shape, BF16),
        in_specs=vmem(3) + [pl.BlockSpec(memory_space=pl.ANY)] * 3,
        out_specs=vmem(1)[0],
        scratch_shapes=[pltpu.VMEM((nt, rows, width), BF16), pltpu.VMEM((rows, width), BF16),
                        dma((nt,)), dma((nt,))]
        + half_scratch(nk, nt, rows, width, gate.shape[0]),
        compiler_params=params(2),
        name="second_half",
    )(own, pout, gain, gate, lift, down)


def conv(taps_ref, buf_ref, newest):
    taps = taps_ref[...].astype(F32)
    count = taps.shape[0]
    old = buf_ref[...].astype(F32)
    acc = newest.astype(BF16).astype(F32) * taps[count - 1 : count]
    for k in range(count - 1):
        acc = acc + old[k] * taps[k : k + 1]
    return silu(acc)


def split(v):
    high = v.astype(BF16).astype(F32)
    return high, v - high


def mixer_kernel(first, gain, wz, wx, wb, wr, ws, bias, rate, skip, tx, tb, tr, bx, bb, br,
                 wo, state, pout, state_out,
                 z_s, x_s, r_s, ho_s, left_s, base_s):
    step_id = pl.program_id(0)
    nt, rows, width = first.shape
    features = nt * width
    chans = wx.shape[1]
    heads = ws.shape[0]
    groups = wb.shape[1] // STATE
    gch = chans // groups
    depth = base_s.shape[1]

    def spread(v):
        r = lax.broadcasted_iota(jnp.int32, (heads, chans), 0)
        c = lax.broadcasted_iota(jnp.int32, (heads, chans), 1)
        ind = jnp.where(c // HEAD_DIM == r, 1.0, 0.0).astype(F32)
        return jnp.dot(v, ind, precision=lax.Precision.HIGHEST, preferred_element_type=F32)

    @pl.when(step_id == 0)
    def _():
        total = jnp.zeros((rows, 1), F32)
        for t in range(nt):
            v = first[t].astype(F32)
            total = total + jnp.sum(v * v, axis=1, keepdims=True)
        factor = lax.rsqrt(total / features + EPS)
        normed = jnp.concatenate(
            [(first[t].astype(F32) * factor
              * gain[:, (t + 3) * width:(t + 4) * width].astype(F32)).astype(BF16)
             for t in range(nt)], axis=1)
        z_s[...] = dot(normed, wz[...]).astype(BF16).astype(F32)
        xc = conv(tx, bx, dot(normed, wx[...]))
        x_s[...] = xc
        bc = conv(tb, bb, dot(normed, wb[...]))
        rc = conv(tr, br, dot(normed, wr[...]))
        for i in range(rows):
            r_s[i] = rc[i:i + 1]
        raw = dot_t(normed, ws[...]).astype(BF16).astype(F32) + bias[...]
        step = jnp.maximum(raw, 0.0) + jnp.log1p(jnp.exp(-jnp.abs(raw)))
        retain = jnp.exp(-step * jnp.exp(rate[...]))
        sx_hi, sx_lo = split(spread(step) * xc)
        re_hi, re_lo = split(spread(retain))
        pad = depth - 5 * rows
        left = jnp.concatenate(
            [sx_hi, sx_lo, sx_hi, re_hi, re_lo, jnp.zeros((pad, chans), F32)], axis=0)
        left_s[...] = left.T.astype(BF16)
        for g in range(groups):
            b_hi, b_lo = split(bc[:, g * STATE:(g + 1) * STATE])
            zero = jnp.zeros((rows, STATE), F32)
            one = jnp.ones((rows, STATE), F32)
            zpad = jnp.zeros((pad, STATE), F32)
            base_s[g, :, :STATE] = jnp.concatenate(
                [b_hi, b_hi, b_lo, zero, zero, zpad], axis=0).astype(BF16)
            base_s[g, :, STATE:] = jnp.concatenate(
                [zero, zero, zero, one, one, zpad], axis=0).astype(BF16)

    block = state.shape[0]
    rowmod = lax.rem(lax.broadcasted_iota(jnp.int32, (depth, 2 * STATE), 0), rows)
    pick = lax.broadcasted_iota(jnp.int32, (16, STATE), 0)
    hg = heads // groups
    for i in range(block):
        b = step_id * block + i
        mask = jnp.where(rowmod == b, 1.0, 0.0).astype(BF16)
        for g in range(groups):
            right = base_s[g] * mask
            both = dot(left_s[g * gch:(g + 1) * gch, :], right)
            old = state[i, g * hg:(g + 1) * hg].reshape(gch, STATE)
            new = both[:, STATE:] * old + both[:, :STATE]
            state_out[i, g * hg:(g + 1) * hg] = new.reshape(hg, HEAD_DIM, STATE)
            r_hi, r_lo = split(r_s[b][:, g * STATE:(g + 1) * STATE])
            rr = jnp.where(pick == 0, r_hi, jnp.where(pick == 1, r_lo, 0.0)).astype(BF16)
            ho = lax.dot_general(rr, new.astype(BF16), (((1,), (1,)), ((), ())),
                                 preferred_element_type=F32)
            ho_s[b, :, g * gch:(g + 1) * gch] = jnp.sum(ho, axis=0, keepdims=True)

    @pl.when(step_id == pl.num_programs(0) - 1)
    def _():
        heads_out = jnp.concatenate([ho_s[i] for i in range(rows)], axis=0)
        out = (heads_out + spread(skip[...]) * x_s[...]).astype(BF16).astype(F32)
        gated = out * silu(z_s[...])
        pieces = []
        for g in range(groups):
            v = gated[:, g * gch:(g + 1) * gch]
            pieces.append(v * lax.rsqrt(jnp.mean(v * v, axis=1, keepdims=True) + EPS))
        gated = (jnp.concatenate(pieces, axis=1) * gain[:, 2 * width:3 * width].astype(F32)).astype(BF16)
        for t in range(nt):
            pout[t] = dot(gated, wo[:, t * width:(t + 1) * width]).astype(BF16)


def mixer(first, gain, wz, wx, wb, wr, ws, bias, rate, skip, tx, tb, tr, bx, bb, br,
          state, wo):
    nt, rows, width = first.shape
    chans, heads = wx.shape[1], ws.shape[0]
    groups = wb.shape[1] // STATE
    depth = -(-5 * rows // 128) * 128
    block = 4 if rows % 4 == 0 else 1
    small = [first, gain, wz, wx, wb, wr, ws, bias[None, :], rate[None, :],
             skip[None, :], tx, tb, tr] + [jnp.transpose(v, (1, 0, 2)) for v in (bx, bb, br)] + [
             wo]

    def whole(v):
        zeros = (0,) * v.ndim
        return pl.BlockSpec(v.shape, lambda i: zeros, pipeline_mode=pl.Buffered(1))

    state_spec = pl.BlockSpec((block,) + state.shape[1:], lambda i: (i, 0, 0, 0))
    return pl.pallas_call(
        mixer_kernel,
        grid=(rows // block,),
        out_shape=(jax.ShapeDtypeStruct(first.shape, BF16),
                   jax.ShapeDtypeStruct(state.shape, F32)),
        in_specs=[whole(v) for v in small] + [state_spec],
        out_specs=(pl.BlockSpec(first.shape, lambda i: (0, 0, 0)), state_spec),
        scratch_shapes=[
            pltpu.VMEM((rows, chans), F32),
            pltpu.VMEM((rows, chans), F32),
            pltpu.VMEM((rows, 1, groups * STATE), F32),
            pltpu.VMEM((rows, 1, chans), F32),
            pltpu.VMEM((chans, depth), BF16),
            pltpu.VMEM((groups, depth, 2 * STATE), BF16),
        ],
        compiler_params=pltpu.CompilerParams(
            vmem_limit_bytes=VMEM_LIMIT, dimension_semantics=("arbitrary",)),
        name="mixer",
    )(*small, state)


def per_device(nk, nt, residual, first_gain, first_gate, first_lift, first_down, *rest):
    mix = list(rest[:18])
    second_gain, second_gate, second_lift, second_down = rest[18:]
    width = residual.shape[1]
    gains = lax.optimization_barrier(
        jnp.concatenate([first_gain, second_gain, mix[16], mix[0]])[None, :])
    mix[0] = gains
    del mix[16]
    mix[5] = mix[5].T
    own, gathered = first_half(
        nk, nt, residual, gains, first_gate.T, first_lift.T, first_down)
    pout, state_out = mixer(gathered, *mix)
    out = second_half(nk, nt, own, pout, gains,
                      second_gate.T, second_lift.T, second_down)
    return (out, state_out)


def solution(mesh):
    placed = (
        P("kv", "tp"),
        P("tp"),
        P("tp", "kv"),
        P("tp", "kv"),
        P("kv", "tp"),
        P(),
        P(None, "tp"),
        P(None, "tp"),
        P(None, "tp"),
        P(None, "tp"),
        P(None, "tp"),
        P("tp"),
        P("tp"),
        P("tp"),
        P(None, "tp"),
        P(None, "tp"),
        P(None, "tp"),
        P("kv", None, "tp"),
        P("kv", None, "tp"),
        P("kv", None, "tp"),
        P("kv", "tp", None, None),
        P("tp"),
        P("tp", None),
        P("tp"),
        P("tp", "kv"),
        P("tp", "kv"),
        P("kv", "tp"),
    )
    return jax.shard_map(
        functools.partial(per_device, mesh.shape["kv"], mesh.shape["tp"]),
        mesh=mesh,
        in_specs=placed,
        out_specs=(P("kv", "tp"), P("kv", "tp", None, None)),
        check_vma=False,
    )
```

profile of v0, /device:TPU:6, one launch (start us, length us, event | category | flops | bytes accessed | tf_op | source)
XLA Modules:
  0.0 103.9 jit_solution(14710509900785564658)
XLA Ops:
  0.6 0.7 pad_maximum_fusion
  1.4 0.6 broadcast_in_dim.12.gain_ref.gain
  2.0 37.1 %first_half.1 = (bf16[32,512]{1,0:T(8,128)(2,1)}, bf16[4,32,512]{2,1,0:T(8,128)(2,1)}) custom-call(bf16[32,512]{1,0:T(8,128)(2,1)} %x_ref.1, bf16[1,3584]{1,0:T(2,128)(2,1)} %broadcast_in_dim.12.gain_ref.gain, bf16[704,512]{1,0:T(8,128)(2,1)} %bitcast.11, bf16[704,512]{1,0:T(8,128)(2,1)} %bitcast.12, bf16[704,512]{1,0:T(8,128)(2,1)} %down.2), custom_call_target="tpu_custom_call" | custom-call | tf_op jit(solution)/shard_map/first_half/pallas_call | solution.py:244
  39.1 23.1 %mixer.1 = (bf16[4,32,512]{2,1,0:T(8,128)(2,1)}, f32[32,8,64,128]{3,2,1,0:T(8,128)}) custom-call(bf16[4,32,512]{2,1,0:T(8,128)(2,1)} %get-tuple-element.7.first, bf16[1,3584]{1,0:T(2,128)(2,1)} %broadcast_in_dim.12.gain_ref.gain, bf16[2048,512]{1,0:T(8,128)(2,1)} %wz.1, bf16[2048,512]{1,0:T(8,128)(2,1)} %wx.1, bf16[2048,256]{1,0:T(8,128)(2,1)} %wb.1, ...), custom_call_target="tpu_custom_call" | custom-call | tf_op jit(solution)/shard_map/mixer/pallas_call | solution.py:392
  62.1 40.4 %second_half.1 = bf16[32,512]{1,0:T(8,128)(2,1)} custom-call(bf16[32,512]{1,0:T(8,128)(2,1)} %get-tuple-element.6.own_ref, bf16[4,32,512]{2,1,0:T(8,128)(2,1)} %get-tuple-element.8.pout_ref, bf16[1,3584]{1,0:T(2,128)(2,1)} %broadcast_in_dim.12.gain_ref.gain, bf16[704,512]{1,0:T(8,128)(2,1)} %bitcast.13, bf16[704,512]{1,0:T(8,128)(2,1)} %bitcast.14, ...), custom_call_target="tpu_custom_call" | custom-call | tf_op jit(solution)/shard_map/second_half/pallas_call | solution.py:260
  102.6 1.4 %copy.30 = bf16[32,512]{1,0:T(8,128)(2,1)} copy(bf16[32,512]{1,0:T(8,128)(2,1)} %second_half.1) | data formatting | bytes 65536
where the time goes:
time: 104 us
  Pallas kernels  101 us (97%)
  local copies, waits for them, and re-layouts  1.99 us (2%)
    pallas_call x1, Pallas kernels, second_half(): pl.pallas_call(functools.partial(second_kernel, nk, nt), out_shape=jax.Sh...  40.4 us
    pallas_call x1, Pallas kernels, first_half(): pl.pallas_call(functools.partial(first_kernel, nk, nt), out_shape=(jax.Sh...  37.1 us
    pallas_call x1, Pallas kernels, mixer(): pl.pallas_call(mixer_kernel, grid=(rows // block,), out_shape=(jax.ShapeD...  23.1 us

commit v1 on v0

v1 whole, which is shorter than its diff:
```python
import functools

import jax
import jax.numpy as jnp
from jax import lax
from jax.experimental import pallas as pl
from jax.experimental.pallas import tpu as pltpu
from jax.sharding import PartitionSpec as P

HEAD_DIM = 64
STATE = 128
EPS = 1e-06
MESH = pl.DeviceIdType.MESH
F32 = jnp.float32
BF16 = jnp.bfloat16
DMA = pltpu.SemaphoreType.DMA


def silu(v):
    return v / (1.0 + jnp.exp(-v))


def dot(a, b):
    return jnp.dot(a, b, preferred_element_type=F32)


def dot_t(a, b, precision=None):
    return lax.dot_general(a, b, (((1,), (1,)), ((), ())), precision=precision,
                           preferred_element_type=F32)


def far_first(n):
    return sorted(range(1, n), key=lambda d: -min(d, n - d))


def remote(src, dst, send, recv, where):
    return pltpu.make_async_remote_copy(
        src_ref=src, dst_ref=dst, send_sem=send, recv_sem=recv,
        device_id=where, device_id_type=MESH,
    )


class Place:
    def __init__(self, nk, nt):
        self.nk, self.nt, self.nx = nk, nt, nt // 2
        self.kv, self.tp = lax.axis_index("kv"), lax.axis_index("tp")
        self.core = lax.rem(self.tp, 2)
        self.x = lax.div(self.tp, 2)
        self.partner = {"tp": self.tp + 1 - 2 * self.core}

    def kv_to(self, d):
        return lax.rem(self.kv + d, self.nk)

    def kv_from(self, d):
        return lax.rem(self.kv + self.nk - d, self.nk)

    def tp_to(self, d):
        return lax.rem(self.tp + d, self.nt)

    def tp_from(self, d):
        return lax.rem(self.tp + self.nt - d, self.nt)

    def x_to(self, e):
        return lax.rem(self.x + e, self.nx)

    def x_from(self, e):
        return lax.rem(self.x + self.nx - e, self.nx)

    def same_core(self, x):
        return {"tp": 2 * x + self.core}


def enter(p):
    barrier = pltpu.get_barrier_semaphore()
    for d in range(1, p.nk):
        pl.semaphore_signal(barrier, inc=1, device_id={"kv": p.kv_to(d)}, device_id_type=MESH)
    for d in range(1, p.nt):
        pl.semaphore_signal(barrier, inc=1, device_id={"tp": p.tp_to(d)}, device_id_type=MESH)
    pl.semaphore_wait(barrier, p.nk + p.nt - 2)


def half_scratch(nk, nt, rows, width, halfc):
    total, nx = nk * rows, nt // 2
    share = total // nx
    vmem = pltpu.VMEM
    return dict(
        wg=vmem((2, halfc, width), BF16), wu=vmem((2, halfc, width), BF16),
        wd=vmem((2, halfc, width), BF16), wl=DMA((4,)), ws=DMA((2,)), wr=DMA((2,)),
        xall=vmem((total, width), BF16), xg=vmem((2, total, width), BF16),
        ssq=vmem((total, 128), F32),
        sq=vmem((nx, 8, share), F32), sqr=vmem((nt, 8, share), F32),
        part=vmem((nx, 2, share, halfc), BF16), parr=vmem((nx, 2, share, halfc), BF16),
        hid=vmem((2, total, halfc), BF16),
        dpart=vmem((total, width), BF16), dparr=vmem((nk, rows, width), BF16),
        ag_s=DMA((nk,)), ag_r=DMA((nk,)), dd_s=DMA((nk,)), dd_r=DMA((nk,)),
        sq_s=DMA((nt,)), sq_r=DMA((nt,)), rs_s=DMA((nx, 2)), rs_r=DMA((nx, 2)),
        hx_s=DMA((nx,)), hx_r=DMA((nx,)), hd_s=DMA((nx,)), hd_r=DMA((nx,)),
        dn_s=DMA((nk,)), dn_r=DMA((nk,)),
    )


def local_weights(p, s, gate, lift, down):
    copies = [
        pltpu.make_async_copy(gate.at[p.core], s["wg"].at[0], s["wl"].at[0]),
        pltpu.make_async_copy(lift.at[p.core], s["wu"].at[0], s["wl"].at[1]),
        pltpu.make_async_copy(down.at[p.core], s["wd"].at[0], s["wl"].at[2]),
        pltpu.make_async_copy(down.at[1 - p.core], s["wd"].at[1], s["wl"].at[3]),
    ]
    for c in copies:
        c.start()
    return copies


def swap_weights(p, s, gate, lift):
    copies = [
        remote(gate.at[1 - p.core], s["wg"].at[1], s["ws"].at[0], s["wr"].at[0], p.partner),
        remote(lift.at[1 - p.core], s["wu"].at[1], s["ws"].at[1], s["wr"].at[1], p.partner),
    ]
    for c in copies:
        c.start()
    return copies


def half_step(p, s, x_ref, gain, local, swapped, idle):
    nk, nt, nx = p.nk, p.nt, p.nx
    rows, width = x_ref.shape
    total = nk * rows
    share = total // nx
    per = share // rows
    features = width * nt
    sends = []

    def block(k):
        return pl.ds(pl.multiple_of(k * rows, rows), rows)

    def part_rows(x):
        return pl.ds(pl.multiple_of(x * share, share), share)

    gathers = {}
    for d in far_first(nk):
        c = remote(x_ref, s["xall"].at[block(p.kv)], s["ag_s"].at[d], s["ag_r"].at[d],
                   {"kv": p.kv_to(d)})
        c.start()
        gathers[d] = c
    sends += gathers.values()
    idle[0]()
    forwards = []
    for d in [0] + list(reversed(far_first(nk))):
        at = block(p.kv_from(d))
        if d:
            gathers[d].wait_recv()
            value = s["xall"][at, :].astype(F32)
        else:
            value = x_ref[...].astype(F32)
        s["xg"][0, at, :] = (value * gain).astype(BF16)
        c = remote(s["xg"].at[0, at], s["xg"].at[1, at], s["dd_s"].at[d], s["dd_r"].at[d],
                   p.partner)
        c.start()
        forwards.append(c)
        value = value * value
        folded = value[:, :128]
        for i in range(128, width, 128):
            folded = folded + value[:, i:i + 128]
        s["ssq"][at, :] = folded
    sends += forwards
    ones = jnp.ones((8, 128), F32)
    for x in range(nx):
        s["sq"][x] = dot_t(ones, s["ssq"][x * share:(x + 1) * share, :], lax.Precision.HIGHEST)
    squares = []
    for d in far_first(nt):
        to = p.tp_to(d)
        c = remote(s["sq"].at[lax.div(to, 2)], s["sqr"].at[d], s["sq_s"].at[d], s["sq_r"].at[d],
                   {"tp": to})
        c.start()
        squares.append((d, c))
    sends += [c for _, c in squares]
    local[0].wait()
    local[1].wait()
    for c in swapped:
        c.wait_recv()
    for c in forwards:
        c.wait_recv()

    def partial(x, w):
        at = part_rows(x)
        return dot_t(s["xg"][0, at, :], w[0]) + dot_t(s["xg"][1, at, :], w[1])

    parts = {}
    for e in far_first(nx):
        to = p.x_to(e)
        for i, w in enumerate((s["wg"], s["wu"])):
            s["part"][e, i] = partial(to, w).astype(BF16)
            c = remote(s["part"].at[e, i], s["parr"].at[e, i], s["rs_s"].at[e, i],
                       s["rs_r"].at[e, i], p.same_core(to))
            c.start()
            parts[e, i] = c
    sends += parts.values()
    gate = partial(p.x, s["wg"])
    lift = partial(p.x, s["wu"])
    s["part"][0, 0] = gate.astype(BF16)
    s["part"][0, 1] = lift.astype(BF16)
    idle[1]()
    sq = s["sq"][p.x]
    for d, c in squares:
        c.wait_recv()
        sq = sq + s["sqr"][d]
    factor = jnp.transpose(lax.rsqrt(sq / features + EPS))[:, :1]
    gate = s["part"][0, 0].astype(F32)
    lift = s["part"][0, 1].astype(F32)
    for e in reversed(far_first(nx)):
        parts[e, 0].wait_recv()
        gate = gate + s["parr"][e, 0].astype(F32)
    gate = silu(gate * factor) * factor
    for e in reversed(far_first(nx)):
        parts[e, 1].wait_recv()
        lift = lift + s["parr"][e, 1].astype(F32)
    mine = part_rows(p.x)
    s["hid"][0, mine, :] = (gate * lift).astype(BF16)
    spread = {}
    for e in far_first(nx):
        c = remote(s["hid"].at[0, mine], s["hid"].at[0, mine], s["hx_s"].at[e], s["hx_r"].at[e],
                   p.same_core(p.x_to(e)))
        c.start()
        spread[e] = c
    sends += spread.values()
    across = {}

    def forward(e):
        at = part_rows(p.x_from(e))
        c = remote(s["hid"].at[0, at], s["hid"].at[1, at], s["hd_s"].at[e], s["hd_r"].at[e],
                   p.partner)
        c.start()
        across[e] = c

    forward(0)
    local[2].wait()
    local[3].wait()
    order = [0] + list(reversed(far_first(nx)))
    for n, e in enumerate(order):
        source = p.x_from(e)
        at = part_rows(source)
        if e:
            spread[e].wait_recv()
            forward(e)
        mid = dot(s["hid"][0, at, :], s["wd"][0])
        across[e].wait_recv()
        s["dpart"][at, :] = (mid + dot(s["hid"][1, at, :], s["wd"][1])).astype(BF16)
        for j in range(per):
            to = source * per + j

            @pl.when(to != p.kv)
            def _():
                remote(s["dpart"].at[block(to)], s["dparr"].at[p.kv], s["dn_s"].at[to],
                       s["dn_r"].at[p.kv], {"kv": to}).start()

        if n == 0:
            idle[2]()
    sends += across.values()
    idle[3]()
    acc = s["dpart"][block(p.kv), :].astype(F32)
    for d in reversed(far_first(nk)):
        source = p.kv_from(d)
        there = s["dparr"].at[source]
        pltpu.make_async_copy(there, there, s["dn_r"].at[source]).wait()
        acc = acc + s["dparr"][source].astype(F32)

    def finish():
        for d in far_first(nk):
            to = p.kv_to(d)
            there = s["dparr"].at[to]
            pltpu.make_async_copy(there, there, s["dn_s"].at[to]).wait()
        for c in sends + swapped:
            c.wait_send()

    return x_ref[...].astype(F32) + 0.5 * acc, finish


def conv(taps_ref, buf_ref, newest):
    taps = taps_ref[...].astype(F32)
    count = taps.shape[0]
    old = buf_ref[...].astype(F32)
    acc = newest.astype(BF16).astype(F32) * taps[count - 1:count]
    for k in range(count - 1):
        acc = acc + old[k] * taps[k:k + 1]
    return silu(acc)


def split(v):
    high = v.astype(BF16).astype(F32)
    return high, v - high


def layer_kernel(nk, nt, names, *refs):
    r = dict(zip(names, refs))
    p = Place(nk, nt)
    one = {k[2:]: v for k, v in r.items() if k.startswith("1.")}
    two = {k[2:]: v for k, v in r.items() if k.startswith("2.")}
    x_ref, state = r["x"], r["state_out"]
    rows, width = x_ref.shape
    features = nt * width
    chans = r["wx"].shape[-1]
    gs = r["wb"].shape[-1]
    heads = r["ws"].shape[0]
    groups = gs // STATE
    gch = chans // groups
    hg = heads // groups
    wcat = r["wcat"]

    local1 = local_weights(p, one, r["gate1"], r["lift1"], r["down1"])
    mixload = []
    at = 0
    for i, name in enumerate(("wz", "wx", "wb", "wr")):
        w = r[name]
        c = pltpu.make_async_copy(w, wcat.at[:, :, at:at + w.shape[-1]], r["ml"].at[i])
        at += w.shape[-1]
        mixload.append(c)
    mixload.append(pltpu.make_async_copy(r["wo"], r["wov"], r["ml"].at[4]))
    stateload = pltpu.make_async_copy(r["state"], state, r["ml"].at[5])
    enter(p)
    swap1 = swap_weights(p, one, r["gate1"], r["lift1"])

    def row(name):
        return r[name][...].astype(F32).reshape(1, -1)

    later = {}

    def load_rest():
        stateload.start()
        for c in mixload:
            c.start()
        later["local"] = local_weights(p, two, r["gate2"], r["lift2"], r["down2"])
        later["swap"] = swap_weights(p, two, r["gate2"], r["lift2"])

    def narrow():
        stateload.wait()

        def body(i, _):
            for g in range(groups):
                pair = [state[2 * i + j, g * hg:(g + 1) * hg].reshape(gch, STATE)
                        for j in range(2)]
                r["stb"][i, g * gch:(g + 1) * gch, :] = jnp.concatenate(pair, axis=1).astype(BF16)
            return 0

        lax.fori_loop(0, rows // 2, body, 0)

    def nothing():
        pass

    first, finish1 = half_step(p, one, x_ref, row("g1"), local1, swap1,
                               (load_rest, narrow, nothing, nothing))
    held = r["held"]
    held[p.tp] = first.astype(BF16)
    copies = {}
    for d in far_first(nt):
        c = remote(held.at[p.tp], held.at[p.tp], r["f_s"].at[d], r["f_r"].at[d],
                   {"tp": p.tp_to(d)})
        c.start()
        copies[d] = c
    for c in mixload:
        c.wait()
    gm = row("gm")
    gmv = r["gmv"]
    for t in range(nt):
        gmv[t] = gm[:, t * width:(t + 1) * width]
    total = jnp.zeros((rows, 1), F32)
    proj = jnp.zeros((rows, wcat.shape[-1]), F32)
    raw = jnp.zeros((rows, heads), F32)
    for d in [0] + list(reversed(far_first(nt))):
        t = p.tp_from(d)
        if d:
            copies[d].wait_recv()
        v = held[t].astype(F32)
        total = total + jnp.sum(v * v, axis=1, keepdims=True)
        scaled = (v * gmv[t]).astype(BF16)
        proj = proj + dot(scaled, wcat[t])
        raw = raw + dot_t(scaled, r["ws"][:, pl.ds(pl.multiple_of(t * width, width), width)])
    factor = lax.rsqrt(total / features + EPS)
    proj = proj * factor
    raw = (raw * factor).astype(BF16).astype(F32) + r["bias"][...]

    def spread(v):
        a = lax.broadcasted_iota(jnp.int32, (heads, chans), 0)
        c = lax.broadcasted_iota(jnp.int32, (heads, chans), 1)
        ind = jnp.where(c // HEAD_DIM == a, 1.0, 0.0).astype(F32)
        return jnp.dot(v, ind, precision=lax.Precision.HIGHEST, preferred_element_type=F32)

    z = proj[:, :chans].astype(BF16).astype(F32)
    xc = conv(r["tx"], r["bx"], proj[:, chans:2 * chans])
    bc = conv(r["tb"], r["bb"], proj[:, 2 * chans:2 * chans + gs])
    rc = conv(r["tr"], r["br"], proj[:, 2 * chans + gs:])
    step = jnp.maximum(raw, 0.0) + jnp.log1p(jnp.exp(-jnp.abs(raw)))
    retain = jnp.exp(-step * jnp.exp(r["rate"][...]))
    sx = spread(step) * xc
    keep = spread(retain)

    rowid = lax.broadcasted_iota(jnp.int32, (rows, 2 * STATE), 0)
    colid = lax.broadcasted_iota(jnp.int32, (rows, 2 * STATE), 1) // STATE
    pieces = []
    for g in range(groups):
        rg = rc[:, g * STATE:(g + 1) * STATE]
        twice = jnp.concatenate([rg, rg], axis=1)
        acc = jnp.zeros((rows, gch), F32)
        for i in range(rows // 2):
            lhs = jnp.where(rowid - colid == 2 * i, twice, 0.0).astype(BF16)
            acc = acc + dot_t(lhs, r["stb"][i, g * gch:(g + 1) * gch, :])
        br = jnp.sum(bc[:, g * STATE:(g + 1) * STATE] * rg, axis=1, keepdims=True)
        pieces.append(acc * keep[:, g * gch:(g + 1) * gch] + sx[:, g * gch:(g + 1) * gch] * br)
    out = jnp.concatenate(pieces, axis=1) + spread(r["skip"][...]) * xc
    gated = out.astype(BF16).astype(F32) * silu(z)
    pieces = []
    for g in range(groups):
        v = gated[:, g * gch:(g + 1) * gch]
        pieces.append(v * lax.rsqrt(jnp.mean(v * v, axis=1, keepdims=True) + EPS))
    gated = (jnp.concatenate(pieces, axis=1) * row("gg")).astype(BF16)
    pout, arrived = r["pout"], r["arrived"]
    outs = {}
    for d in far_first(nt) + [0]:
        to = p.tp_to(d)
        wo = r["wov"][:, pl.ds(pl.multiple_of(to * width, width), width)]
        pout[d] = dot(gated, wo).astype(BF16)
        if d:
            c = remote(pout.at[d], arrived.at[d], r["m_s"].at[d], r["m_r"].at[d], {"tp": to})
            c.start()
            outs[d] = c

    depth = r["base"].shape[1]
    pad = depth - 5 * rows
    sx_hi, sx_lo = split(sx)
    re_hi, re_lo = split(keep)
    left = jnp.concatenate(
        [sx_hi, sx_lo, sx_hi, re_hi, re_lo, jnp.zeros((pad, chans), F32)], axis=0)
    r["left"][...] = left.T.astype(BF16)
    for g in range(groups):
        b_hi, b_lo = split(bc[:, g * STATE:(g + 1) * STATE])
        zero = jnp.zeros((rows, STATE), F32)
        full = jnp.ones((rows, STATE), F32)
        zpad = jnp.zeros((pad, STATE), F32)
        r["base"][g, :, :STATE] = jnp.concatenate(
            [b_hi, b_hi, b_lo, zero, zero, zpad], axis=0).astype(BF16)
        r["base"][g, :, STATE:] = jnp.concatenate(
            [zero, zero, zero, full, full, zpad], axis=0).astype(BF16)

    acc = held[p.tp].astype(F32) + pout[0].astype(F32)
    for d in reversed(far_first(nt)):
        outs[d].wait_recv()
        acc = acc + arrived[d].astype(F32)
    r["mixed"][...] = acc.astype(BF16)

    rowmod = lax.rem(lax.broadcasted_iota(jnp.int32, (depth, 2 * STATE), 0), rows)

    def update(low, high):
        def body(b, _):
            mask = jnp.where(rowmod == b, 1.0, 0.0).astype(BF16)
            for g in range(groups):
                right = r["base"][g] * mask
                both = dot(r["left"][g * gch:(g + 1) * gch, :], right)
                old = state[b, g * hg:(g + 1) * hg].reshape(gch, STATE)
                new = both[:, STATE:] * old + both[:, :STATE]
                state[b, g * hg:(g + 1) * hg] = new.reshape(hg, HEAD_DIM, STATE)
            return 0

        return lambda: lax.fori_loop(low, high, body, 0)

    last, finish2 = half_step(p, two, r["mixed"], row("g2"), later["local"], later["swap"],
                              (update(0, rows // 2), update(rows // 2, rows), nothing, nothing))
    r["out"][...] = last.astype(BF16)
    finish1()
    finish2()
    for c in list(copies.values()) + list(outs.values()):
        c.wait_send()


def flush_kernel(a, b, oa, ob, sem):
    copies = [pltpu.make_async_copy(a, oa, sem.at[0]), pltpu.make_async_copy(b, ob, sem.at[1])]
    for c in copies:
        c.start()
    for c in copies:
        c.wait()


def per_device(nk, nt, residual, first_gain, first_gate, first_lift, first_down,
               mixer_gain, wz, wx, wb, wr, ws, bias, rate, skip, tx, tb, tr, bx, bb, br,
               state, group_gain, wo, second_gain, second_gate, second_lift, second_down):
    rows, width = residual.shape
    halfc = first_gate.shape[1] // 2
    chans, heads = wx.shape[1], ws.shape[1]
    groups = wb.shape[1] // STATE
    vmem = pltpu.VMEM

    def tall(w):
        return w.T.reshape(2, halfc, width)

    def flip(v):
        return jnp.transpose(v, (1, 0, 2))

    small = dict(x=residual, g1=first_gain, g2=second_gain, gm=mixer_gain, gg=group_gain,
                 ws=ws.T, bias=bias[None, :], rate=rate[None, :], skip=skip[None, :],
                 tx=tx, tb=tb, tr=tr, bx=flip(bx), bb=flip(bb), br=flip(br))
    big = dict(gate1=tall(first_gate), lift1=tall(first_lift),
               down1=first_down.reshape(2, halfc, width),
               gate2=tall(second_gate), lift2=tall(second_lift),
               down2=second_down.reshape(2, halfc, width),
               wz=wz.reshape(nt, width, -1), wx=wx.reshape(nt, width, -1),
               wb=wb.reshape(nt, width, -1), wr=wr.reshape(nt, width, -1), wo=wo, state=state)
    depth = -(-5 * rows // 128) * 128
    scratch = dict(
        wcat=vmem((nt, width, 2 * chans + 2 * groups * STATE), BF16),
        wov=vmem(wo.shape, BF16), ml=DMA((6,)),
        stb=vmem((rows // 2, chans, 2 * STATE), BF16),
        held=vmem((nt, rows, width), BF16), f_s=DMA((nt,)), f_r=DMA((nt,)),
        gmv=vmem((nt, 1, width), F32),
        pout=vmem((nt, rows, width), BF16), arrived=vmem((nt, rows, width), BF16),
        m_s=DMA((nt,)), m_r=DMA((nt,)), mixed=vmem((rows, width), BF16),
        left=vmem((chans, depth), BF16), base=vmem((groups, depth, 2 * STATE), BF16),
    )
    for tag in ("1.", "2."):
        for k, v in half_scratch(nk, nt, rows, width, halfc).items():
            scratch[tag + k] = v
    names = list(small) + list(big) + ["out", "state_out"] + list(scratch)
    inside = pl.BlockSpec(memory_space=pltpu.VMEM)
    outside = pl.BlockSpec(memory_space=pl.ANY)
    out, state_out = pl.pallas_call(
        functools.partial(layer_kernel, nk, nt, names),
        out_shape=(vmem(residual.shape, BF16), vmem(state.shape, F32)),
        in_specs=[inside] * len(small) + [outside] * len(big),
        out_specs=(inside, inside),
        scratch_shapes=list(scratch.values()),
        compiler_params=pltpu.CompilerParams(
            collective_id=1, has_side_effects=True, vmem_limit_bytes=48 * 1024 * 1024),
        name="layer",
    )(*small.values(), *big.values())
    return pl.pallas_call(
        flush_kernel,
        out_shape=(jax.ShapeDtypeStruct(residual.shape, BF16),
                   jax.ShapeDtypeStruct(state.shape, F32)),
        in_specs=[inside] * 2,
        out_specs=(outside, outside),
        scratch_shapes=[DMA((2,))],
        compiler_params=pltpu.CompilerParams(vmem_limit_bytes=1024 * 1024),
        name="flush",
    )(out, state_out)


def solution(mesh):
    placed = (
        P("kv", "tp"),
        P("tp"),
        P("tp", "kv"),
        P("tp", "kv"),
        P("kv", "tp"),
        P(),
        P(None, "tp"),
        P(None, "tp"),
        P(None, "tp"),
        P(None, "tp"),
        P(None, "tp"),
        P("tp"),
        P("tp"),
        P("tp"),
        P(None, "tp"),
        P(None, "tp"),
        P(None, "tp"),
        P("kv", None, "tp"),
        P("kv", None, "tp"),
        P("kv", None, "tp"),
        P("kv", "tp", None, None),
        P("tp"),
        P("tp", None),
        P("tp"),
        P("tp", "kv"),
        P("tp", "kv"),
        P("kv", "tp"),
    )
    return jax.shard_map(
        functools.partial(per_device, mesh.shape["kv"], mesh.shape["tp"]),
        mesh=mesh,
        in_specs=placed,
        out_specs=(P("kv", "tp"), P("kv", "tp", None, None)),
        check_vma=False,
    )
```

time: 104 us -> 75.3 us (0.72)
  the two profiles are of different devices: /device:TPU:6 before, /device:TPU:15 now
where the time goes in v1:
time: 75.3 us; the launch traced here: 75.1 us
  Pallas kernels  74.5 us (99%)
    pallas_call x1, Pallas kernels, per_device(): pl.pallas_call(functools.partial(layer_kernel, nk, nt, names), out_shape=...  71.1 us
    pallas_call x1, Pallas kernels, per_device(): pl.pallas_call(flush_kernel, out_shape=(jax.ShapeDtypeStruct(residual.sha...  3.43 us

profile of v1, /device:TPU:15, one launch (start us, length us, event | category | flops | bytes accessed | tf_op | source)
XLA Modules:
  0.0 75.1 jit_solution(15858142320156202036)
XLA Ops:
  0.6 71.1 %layer.1 = (bf16[32,512]{1,0:T(8,128)(2,1)S(1)}, f32[32,8,64,128]{3,2,1,0:T(8,128)S(1)}) custom-call(bf16[32,512]{1,0:T(8,128)(2,1)} %refs_0_.1, bf16[512]{0:T(512)(128)(2,1)} %refs_1_.1, bf16[512]{0:T(512)(128)(2,1)} %refs_2_.1, bf16[2048]{0:T(1024)(128)(2,1)} %refs_3_.1, bf16[512]{0:T(512)(128)(2,1)} %refs_4_.1, bf16[8,2048]{1,0:T(8,128)(2,1)} %bitcast.38, ...), custom_call_target="tpu_custom_call" | custom-call | tf_op jit(solution)/shard_map/layer/pallas_call | solution.py:522
  71.7 3.4 %flush.1 = (bf16[32,512]{1,0:T(8,128)(2,1)}, f32[32,8,64,128]{3,2,1,0:T(8,128)}) custom-call(bf16[32,512]{1,0:T(8,128)(2,1)S(1)} %get-tuple-element.4.a, f32[32,8,64,128]{3,2,1,0:T(8,128)S(1)} %get-tuple-element.5.b), custom_call_target="tpu_custom_call" | custom-call | tf_op jit(solution)/shard_map/flush/pallas_call | solution.py:532

commit v2 on v1

--- a/solution.py
+++ b/solution.py
@@ -69,6 +69,9 @@
     def same_core(self, x):
         return {"tp": 2 * x + self.core}
 
+    def cross_core(self, x):
+        return {"tp": 2 * x + 1 - self.core}
+
 
 def enter(p):
     barrier = pltpu.get_barrier_semaphore()
@@ -81,20 +84,22 @@
 
 def half_scratch(nk, nt, rows, width, halfc):
     total, nx = nk * rows, nt // 2
-    share = total // nx
+    chunks, size = nk // nx, rows
     vmem = pltpu.VMEM
     return dict(
         wg=vmem((2, halfc, width), BF16), wu=vmem((2, halfc, width), BF16),
         wd=vmem((2, halfc, width), BF16), wl=DMA((4,)), ws=DMA((2,)), wr=DMA((2,)),
         xall=vmem((total, width), BF16), xg=vmem((2, total, width), BF16),
-        ssq=vmem((total, 128), F32),
-        sq=vmem((nx, 8, share), F32), sqr=vmem((nt, 8, share), F32),
-        part=vmem((nx, 2, share, halfc), BF16), parr=vmem((nx, 2, share, halfc), BF16),
+        sq=vmem((nx, chunks, 8, size), F32), sqr=vmem((nt, chunks, 8, size), F32),
+        part=vmem((nx, chunks, 2, size, halfc), BF16),
+        parr=vmem((nx, chunks, 2, size, halfc), BF16),
+        mine=vmem((2, nk // nx * rows, halfc), F32),
         hid=vmem((2, total, halfc), BF16),
         dpart=vmem((total, width), BF16), dparr=vmem((nk, rows, width), BF16),
         ag_s=DMA((nk,)), ag_r=DMA((nk,)), dd_s=DMA((nk,)), dd_r=DMA((nk,)),
-        sq_s=DMA((nt,)), sq_r=DMA((nt,)), rs_s=DMA((nx, 2)), rs_r=DMA((nx, 2)),
-        hx_s=DMA((nx,)), hx_r=DMA((nx,)), hd_s=DMA((nx,)), hd_r=DMA((nx,)),
+        sq_s=DMA((nt, chunks)), sq_r=DMA((nt, chunks)),
+        rs_s=DMA((nx, chunks)), rs_r=DMA((nx, chunks)),
+        hx_s=DMA((nx, 2, chunks)), hx_r=DMA((nx, 2, chunks)),
         dn_s=DMA((nk,)), dn_r=DMA((nk,)),
     )
 
@@ -121,154 +126,162 @@
     return copies
 
 
-def half_step(p, s, x_ref, gain, local, swapped, idle):
+def flip_bits(v, m):
+    out, bit = v, 1
+    while bit <= m:
+        if m & bit:
+            out = out + bit * (1 - 2 * lax.rem(lax.div(v, bit), 2))
+        bit *= 2
+    return out
+
+
+def half_step(p, s, x_ref, gain, local, swapped, idle, tag=''):
     nk, nt, nx = p.nk, p.nt, p.nx
     rows, width = x_ref.shape
-    total = nk * rows
-    share = total // nx
-    per = share // rows
+    per = nk // nx
+    chunks, size = per, rows
     features = width * nt
+    near = lax.div(p.kv, nx)
+    order = [flip_bits(near, i) for i in range(chunks)]
+    peers = far_first(nx)
     sends = []
 
     def block(k):
-        return pl.ds(pl.multiple_of(k * rows, rows), rows)
-
-    def part_rows(x):
-        return pl.ds(pl.multiple_of(x * share, share), share)
-
-    gathers = {}
-    for d in far_first(nk):
-        c = remote(x_ref, s["xall"].at[block(p.kv)], s["ag_s"].at[d], s["ag_r"].at[d],
-                   {"kv": p.kv_to(d)})
+        spot = lax.rem(k, nx) * per + lax.div(k, nx)
+        return pl.ds(pl.multiple_of(spot * rows, rows), rows)
+
+    def chunk(x, i):
+        return pl.ds(pl.multiple_of((x * per + order[i]) * rows, size), size)
+
+    def member(x, i):
+        return order[i] * nx + x
+    for m in range(1, nk):
+        c = remote(x_ref, s["xall"].at[block(p.kv)], s["ag_s"].at[m], s["ag_r"].at[p.kv],
+                   {"kv": flip_bits(p.kv, m)})
         c.start()
-        gathers[d] = c
-    sends += gathers.values()
+        sends.append(c)
+    s["xall"][block(p.kv), :] = x_ref[...]
     idle[0]()
-    forwards = []
-    for d in [0] + list(reversed(far_first(nk))):
-        at = block(p.kv_from(d))
-        if d:
-            gathers[d].wait_recv()
-            value = s["xall"][at, :].astype(F32)
-        else:
-            value = x_ref[...].astype(F32)
+
+    def landed(ref, sem):
+        pltpu.make_async_copy(ref, ref, sem).wait()
+
+    def arrive(k):
+        at = block(k)
+
+        @pl.when(k != p.kv)
+        def _():
+            landed(s["xall"].at[at], s["ag_r"].at[k])
+
+        value = s["xall"][at, :].astype(F32)
         s["xg"][0, at, :] = (value * gain).astype(BF16)
-        c = remote(s["xg"].at[0, at], s["xg"].at[1, at], s["dd_s"].at[d], s["dd_r"].at[d],
-                   p.partner)
-        c.start()
-        forwards.append(c)
+        remote(s["xg"].at[0, at], s["xg"].at[1, at], s["dd_s"].at[k], s["dd_r"].at[k],
+               p.partner).start()
         value = value * value
         folded = value[:, :128]
         for i in range(128, width, 128):
             folded = folded + value[:, i:i + 128]
-        s["ssq"][at, :] = folded
-    sends += forwards
-    ones = jnp.ones((8, 128), F32)
-    for x in range(nx):
-        s["sq"][x] = dot_t(ones, s["ssq"][x * share:(x + 1) * share, :], lax.Precision.HIGHEST)
-    squares = []
-    for d in far_first(nt):
-        to = p.tp_to(d)
-        c = remote(s["sq"].at[lax.div(to, 2)], s["sqr"].at[d], s["sq_s"].at[d], s["sq_r"].at[d],
-                   {"tp": to})
-        c.start()
-        squares.append((d, c))
-    sends += [c for _, c in squares]
-    local[0].wait()
-    local[1].wait()
-    for c in swapped:
-        c.wait_recv()
-    for c in forwards:
-        c.wait_recv()
-
-    def partial(x, w):
-        at = part_rows(x)
-        return dot_t(s["xg"][0, at, :], w[0]) + dot_t(s["xg"][1, at, :], w[1])
-
-    parts = {}
-    for e in far_first(nx):
-        to = p.x_to(e)
-        for i, w in enumerate((s["wg"], s["wu"])):
-            s["part"][e, i] = partial(to, w).astype(BF16)
+        return jnp.broadcast_to(jnp.sum(jnp.transpose(folded), axis=0, keepdims=True), (8, rows))
+
+    def ready(k):
+        landed(s["xg"].at[1, block(k)], s["dd_r"].at[k])
+
+    squares, parts = {}, {}
+
+    def collect(i):
+        for e in peers + [0]:
+            to = p.x_to(e)
+            s["sq"][e, i] = arrive(member(to, i))
+            for other in range(2):
+                if e or other:
+                    where = p.same_core(to) if not other else p.cross_core(to)
+                    c = remote(s["sq"].at[e, i], s["sqr"].at[2 * e + other, i],
+                               s["sq_s"].at[2 * e + other, i], s["sq_r"].at[2 * e + other, i],
+                               where)
+                    c.start()
+                    squares[2 * e + other, i] = c
+    collect(0)
+    for i in range(chunks):
+        if i + 1 < chunks:
+            collect(i + 1)
+        if i == 0:
+            local[0].wait()
+            local[1].wait()
+            for c in swapped:
+                c.wait_recv()
+        for e in peers:
+            to = p.x_to(e)
+            ready(member(to, i))
+            at = chunk(to, i)
+            for j, w in enumerate((s["wg"], s["wu"])):
+                s["part"][e, i, j] = (dot_t(s["xg"][0, at, :], w[0])
+                                      + dot_t(s["xg"][1, at, :], w[1])).astype(BF16)
             c = remote(s["part"].at[e, i], s["parr"].at[e, i], s["rs_s"].at[e, i],
                        s["rs_r"].at[e, i], p.same_core(to))
             c.start()
             parts[e, i] = c
-    sends += parts.values()
-    gate = partial(p.x, s["wg"])
-    lift = partial(p.x, s["wu"])
-    s["part"][0, 0] = gate.astype(BF16)
-    s["part"][0, 1] = lift.astype(BF16)
+    for i in range(chunks):
+        ready(member(p.x, i))
+    whole = pl.ds(pl.multiple_of(p.x * per * rows, rows), per * rows)
+    for j, w in enumerate((s["wg"], s["wu"])):
+        s["mine"][j] = dot_t(s["xg"][0, whole, :], w[0]) + dot_t(s["xg"][1, whole, :], w[1])
+    sends += list(squares.values()) + list(parts.values())
     idle[1]()
-    sq = s["sq"][p.x]
-    for d, c in squares:
-        c.wait_recv()
-        sq = sq + s["sqr"][d]
-    factor = jnp.transpose(lax.rsqrt(sq / features + EPS))[:, :1]
-    gate = s["part"][0, 0].astype(F32)
-    lift = s["part"][0, 1].astype(F32)
-    for e in reversed(far_first(nx)):
-        parts[e, 0].wait_recv()
-        gate = gate + s["parr"][e, 0].astype(F32)
-    gate = silu(gate * factor) * factor
-    for e in reversed(far_first(nx)):
-        parts[e, 1].wait_recv()
-        lift = lift + s["parr"][e, 1].astype(F32)
-    mine = part_rows(p.x)
-    s["hid"][0, mine, :] = (gate * lift).astype(BF16)
     spread = {}
-    for e in far_first(nx):
-        c = remote(s["hid"].at[0, mine], s["hid"].at[0, mine], s["hx_s"].at[e], s["hx_r"].at[e],
-                   p.same_core(p.x_to(e)))
-        c.start()
-        spread[e] = c
+    for i in range(chunks):
+        sq = s["sq"][0, i]
+        for n in range(1, nt):
+            squares[n, i].wait_recv()
+            sq = sq + s["sqr"][n, i]
+        factor = jnp.transpose(lax.rsqrt(sq / features + EPS))[:, :1]
+        own = pl.ds(pl.multiple_of(order[i] * rows, rows), rows)
+        gate, lift = s["mine"][0, own, :], s["mine"][1, own, :]
+        for e in reversed(peers):
+            parts[e, i].wait_recv()
+            gate = gate + s["parr"][e, i, 0].astype(F32)
+            lift = lift + s["parr"][e, i, 1].astype(F32)
+        at = chunk(p.x, i)
+        s["hid"][0, at, :] = (silu(gate * factor) * (lift * factor)).astype(BF16)
+        for e in peers + [0]:
+            for other in range(2):
+                if e or other:
+                    to = p.x_to(e)
+                    where = p.same_core(to) if not other else p.cross_core(to)
+                    c = remote(s["hid"].at[0, at], s["hid"].at[other, at],
+                               s["hx_s"].at[e, other, i], s["hx_r"].at[e, other, i], where)
+                    c.start()
+                    spread[e, other, i] = c
     sends += spread.values()
-    across = {}
-
-    def forward(e):
-        at = part_rows(p.x_from(e))
-        c = remote(s["hid"].at[0, at], s["hid"].at[1, at], s["hd_s"].at[e], s["hd_r"].at[e],
-                   p.partner)
-        c.start()
-        across[e] = c
-
-    forward(0)
+    idle[2]()
     local[2].wait()
     local[3].wait()
-    order = [0] + list(reversed(far_first(nx)))
-    for n, e in enumerate(order):
+    for e in [0] + list(reversed(peers)):
         source = p.x_from(e)
-        at = part_rows(source)
-        if e:
-            spread[e].wait_recv()
-            forward(e)
-        mid = dot(s["hid"][0, at, :], s["wd"][0])
-        across[e].wait_recv()
-        s["dpart"][at, :] = (mid + dot(s["hid"][1, at, :], s["wd"][1])).astype(BF16)
-        for j in range(per):
-            to = source * per + j
+        for i in range(chunks):
+            at = chunk(source, i)
+            if e:
+                spread[e, 0, i].wait_recv()
+            spread[e, 1, i].wait_recv()
+            mid = dot(s["hid"][0, at, :], s["wd"][0]) + dot(s["hid"][1, at, :], s["wd"][1])
+            s["dpart"][at, :] = mid.astype(BF16)
+            to = member(source, i)
 
             @pl.when(to != p.kv)
             def _():
                 remote(s["dpart"].at[block(to)], s["dparr"].at[p.kv], s["dn_s"].at[to],
                        s["dn_r"].at[p.kv], {"kv": to}).start()
-
-        if n == 0:
-            idle[2]()
-    sends += across.values()
     idle[3]()
     acc = s["dpart"][block(p.kv), :].astype(F32)
-    for d in reversed(far_first(nk)):
-        source = p.kv_from(d)
-        there = s["dparr"].at[source]
-        pltpu.make_async_copy(there, there, s["dn_r"].at[source]).wait()
+    for m in range(1, nk):
+        source = flip_bits(p.kv, m)
+        landed(s["dparr"].at[source], s["dn_r"].at[source])
         acc = acc + s["dparr"][source].astype(F32)
-
     def finish():
-        for d in far_first(nk):
-            to = p.kv_to(d)
-            there = s["dparr"].at[to]
-            pltpu.make_async_copy(there, there, s["dn_s"].at[to]).wait()
+        for m in range(1, nk):
+            to = flip_bits(p.kv, m)
+            landed(s["dparr"].at[to], s["dn_s"].at[to])
+        for k in range(nk):
+            landed(s["xg"].at[1, block(k)], s["dd_s"].at[k])
         for c in sends + swapped:
             c.wait_send()
 
@@ -290,12 +303,19 @@
     return high, v - high
 
 
-def layer_kernel(nk, nt, names, *refs):
+def layer_kernel(nk, nt, names, small, *refs):
+    tag = 'k_'
     r = dict(zip(names, refs))
     p = Place(nk, nt)
     one = {k[2:]: v for k, v in r.items() if k.startswith("1.")}
     two = {k[2:]: v for k, v in r.items() if k.startswith("2.")}
-    x_ref, state = r["x"], r["state_out"]
+    state = r["state_out"]
+    smalls = {}
+    for i, name in enumerate(small):
+        smalls[name] = pltpu.make_async_copy(r[name], r["v." + name], r["sl"].at[i])
+        smalls[name].start()
+        r[name] = r["v." + name]
+    x_ref = r["x"]
     rows, width = x_ref.shape
     features = nt * width
     chans = r["wx"].shape[-1]
@@ -305,7 +325,6 @@
     gch = chans // groups
     hg = heads // groups
     wcat = r["wcat"]
-
     local1 = local_weights(p, one, r["gate1"], r["lift1"], r["down1"])
     mixload = []
     at = 0
@@ -317,6 +336,8 @@
     mixload.append(pltpu.make_async_copy(r["wo"], r["wov"], r["ml"].at[4]))
     stateload = pltpu.make_async_copy(r["state"], state, r["ml"].at[5])
     enter(p)
+    smalls["x"].wait()
+    smalls["g1"].wait()
     swap1 = swap_weights(p, one, r["gate1"], r["lift1"])
 
     def row(name):
@@ -347,7 +368,7 @@
         pass
 
     first, finish1 = half_step(p, one, x_ref, row("g1"), local1, swap1,
-                               (load_rest, narrow, nothing, nothing))
+                               (load_rest, narrow, nothing, nothing), 'a_')
     held = r["held"]
     held[p.tp] = first.astype(BF16)
     copies = {}
@@ -358,6 +379,8 @@
         copies[d] = c
     for c in mixload:
         c.wait()
+    for name in small[2:]:
+        smalls[name].wait()
     gm = row("gm")
     gmv = r["gmv"]
     for t in range(nt):
@@ -392,7 +415,6 @@
     retain = jnp.exp(-step * jnp.exp(r["rate"][...]))
     sx = spread(step) * xc
     keep = spread(retain)
-
     rowid = lax.broadcasted_iota(jnp.int32, (rows, 2 * STATE), 0)
     colid = lax.broadcasted_iota(jnp.int32, (rows, 2 * STATE), 1) // STATE
     pieces = []
@@ -422,7 +444,6 @@
             c = remote(pout.at[d], arrived.at[d], r["m_s"].at[d], r["m_r"].at[d], {"tp": to})
             c.start()
             outs[d] = c
-
     depth = r["base"].shape[1]
     pad = depth - 5 * rows
     sx_hi, sx_lo = split(sx)
@@ -439,7 +460,6 @@
             [b_hi, b_hi, b_lo, zero, zero, zpad], axis=0).astype(BF16)
         r["base"][g, :, STATE:] = jnp.concatenate(
             [zero, zero, zero, full, full, zpad], axis=0).astype(BF16)
-
     acc = held[p.tp].astype(F32) + pout[0].astype(F32)
     for d in reversed(far_first(nt)):
         outs[d].wait_recv()
@@ -461,8 +481,10 @@
 
         return lambda: lax.fori_loop(low, high, body, 0)
 
+    cuts = (rows * 3 // 8, rows * 5 // 8)
     last, finish2 = half_step(p, two, r["mixed"], row("g2"), later["local"], later["swap"],
-                              (update(0, rows // 2), update(rows // 2, rows), nothing, nothing))
+                              (update(0, cuts[0]), nothing, update(cuts[0], cuts[1]),
+                               update(cuts[1], rows)), 'b_')
     r["out"][...] = last.astype(BF16)
     finish1()
     finish2()
@@ -471,7 +493,12 @@
 
 
 def flush_kernel(a, b, oa, ob, sem):
-    copies = [pltpu.make_async_copy(a, oa, sem.at[0]), pltpu.make_async_copy(b, ob, sem.at[1])]
+    pieces = sem.shape[0] - 1
+    step = b.shape[0] // pieces
+    copies = [pltpu.make_async_copy(a, oa, sem.at[pieces])]
+    for i in range(pieces):
+        at = pl.ds(i * step, step)
+        copies.append(pltpu.make_async_copy(b.at[at], ob.at[at], sem.at[i]))
     for c in copies:
         c.start()
     for c in copies:
@@ -513,6 +540,9 @@
         m_s=DMA((nt,)), m_r=DMA((nt,)), mixed=vmem((rows, width), BF16),
         left=vmem((chans, depth), BF16), base=vmem((groups, depth, 2 * STATE), BF16),
     )
+    scratch["sl"] = DMA((len(small),))
+    for k, v in small.items():
+        scratch["v." + k] = vmem(v.shape, v.dtype)
     for tag in ("1.", "2."):
         for k, v in half_scratch(nk, nt, rows, width, halfc).items():
             scratch[tag + k] = v
@@ -520,9 +550,9 @@
     inside = pl.BlockSpec(memory_space=pltpu.VMEM)
     outside = pl.BlockSpec(memory_space=pl.ANY)
     out, state_out = pl.pallas_call(
-        functools.partial(layer_kernel, nk, nt, names),
+        functools.partial(layer_kernel, nk, nt, names, list(small)),
         out_shape=(vmem(residual.shape, BF16), vmem(state.shape, F32)),
-        in_specs=[inside] * len(small) + [outside] * len(big),
+        in_specs=[outside] * (len(small) + len(big)),
         out_specs=(inside, inside),
         scratch_shapes=list(scratch.values()),
         compiler_params=pltpu.CompilerParams(
@@ -535,7 +565,7 @@
                    jax.ShapeDtypeStruct(state.shape, F32)),
         in_specs=[inside] * 2,
         out_specs=(outside, outside),
-        scratch_shapes=[DMA((2,))],
+        scratch_shapes=[DMA((9,))],
         compiler_params=pltpu.CompilerParams(vmem_limit_bytes=1024 * 1024),
         name="flush",
     )(out, state_out)

time: 75.3 us -> 65.4 us (0.87)
  the two profiles are of different devices: /device:TPU:15 before, /device:TPU:0 now
where the time goes in v2:
time: 65.4 us; the launch traced here: 65.2 us
  Pallas kernels  64.6 us (99%)
    pallas_call x1, Pallas kernels, per_device(): pl.pallas_call(functools.partial(layer_kernel, nk, nt, names, list(small)...  61.2 us
    pallas_call x1, Pallas kernels, per_device(): pl.pallas_call(flush_kernel, out_shape=(jax.ShapeDtypeStruct(residual.sha...  3.39 us

profile of v2, /device:TPU:0, one launch (start us, length us, event | category | flops | bytes accessed | tf_op | source)
XLA Modules:
  0.0 65.2 jit_solution(13912967613904836195)
XLA Ops:
  0.6 61.2 %layer.1 = (bf16[32,512]{1,0:T(8,128)(2,1)S(1)}, f32[32,8,64,128]{3,2,1,0:T(8,128)S(1)}) custom-call(bf16[32,512]{1,0:T(8,128)(2,1)} %refs_0_.1, bf16[512]{0:T(512)(128)(2,1)} %refs_1_.1, bf16[512]{0:T(512)(128)(2,1)} %refs_2_.1, bf16[2048]{0:T(1024)(128)(2,1)} %refs_3_.1, bf16[512]{0:T(512)(128)(2,1)} %refs_4_.1, bf16[8,2048]{1,0:T(8,128)(2,1)} %bitcast.38, ...), custom_call_target="tpu_custom_call" | custom-call | tf_op jit(solution)/shard_map/layer/pallas_call | solution.py:552
  61.8 3.4 %flush.1 = (bf16[32,512]{1,0:T(8,128)(2,1)}, f32[32,8,64,128]{3,2,1,0:T(8,128)}) custom-call(bf16[32,512]{1,0:T(8,128)(2,1)S(1)} %get-tuple-element.4.a, f32[32,8,64,128]{3,2,1,0:T(8,128)S(1)} %get-tuple-element.5.b), custom_call_target="tpu_custom_call" | custom-call | tf_op jit(solution)/shard_map/flush/pallas_call | solution.py:562

commit v3 on v2

--- a/solution.py
+++ b/solution.py
@@ -252,11 +252,12 @@
                     c.start()
                     spread[e, other, i] = c
     sends += spread.values()
-    idle[2]()
     local[2].wait()
     local[3].wait()
     for e in [0] + list(reversed(peers)):
         source = p.x_from(e)
+        if e == (peers or [0])[-1]:
+            idle[2]()
         for i in range(chunks):
             at = chunk(source, i)
             if e:
@@ -335,6 +336,7 @@
         mixload.append(c)
     mixload.append(pltpu.make_async_copy(r["wo"], r["wov"], r["ml"].at[4]))
     stateload = pltpu.make_async_copy(r["state"], state, r["ml"].at[5])
+    stateload.start()
     enter(p)
     smalls["x"].wait()
     smalls["g1"].wait()
@@ -346,29 +348,31 @@
     later = {}
 
     def load_rest():
-        stateload.start()
         for c in mixload:
             c.start()
         later["local"] = local_weights(p, two, r["gate2"], r["lift2"], r["down2"])
-        later["swap"] = swap_weights(p, two, r["gate2"], r["lift2"])
+        narrow()
 
     def narrow():
         stateload.wait()
 
         def body(i, _):
             for g in range(groups):
-                pair = [state[2 * i + j, g * hg:(g + 1) * hg].reshape(gch, STATE)
-                        for j in range(2)]
-                r["stb"][i, g * gch:(g + 1) * gch, :] = jnp.concatenate(pair, axis=1).astype(BF16)
+                for j in range(2):
+                    old = state[2 * i + j, g * hg:(g + 1) * hg].reshape(gch, STATE)
+                    r["stb"][i, g, j * STATE:(j + 1) * STATE, :] = jnp.transpose(old).astype(BF16)
             return 0
 
         lax.fori_loop(0, rows // 2, body, 0)
+
+    def swap_rest():
+        later["swap"] = swap_weights(p, two, r["gate2"], r["lift2"])
 
     def nothing():
         pass
 
     first, finish1 = half_step(p, one, x_ref, row("g1"), local1, swap1,
-                               (load_rest, narrow, nothing, nothing), 'a_')
+                               (load_rest, swap_rest, nothing, nothing), 'a_')
     held = r["held"]
     held[p.tp] = first.astype(BF16)
     copies = {}
@@ -424,7 +428,7 @@
         acc = jnp.zeros((rows, gch), F32)
         for i in range(rows // 2):
             lhs = jnp.where(rowid - colid == 2 * i, twice, 0.0).astype(BF16)
-            acc = acc + dot_t(lhs, r["stb"][i, g * gch:(g + 1) * gch, :])
+            acc = acc + dot(lhs, r["stb"][i, g])
         br = jnp.sum(bc[:, g * STATE:(g + 1) * STATE] * rg, axis=1, keepdims=True)
         pieces.append(acc * keep[:, g * gch:(g + 1) * gch] + sx[:, g * gch:(g + 1) * gch] * br)
     out = jnp.concatenate(pieces, axis=1) + spread(r["skip"][...]) * xc
@@ -445,21 +449,17 @@
             c.start()
             outs[d] = c
     depth = r["base"].shape[1]
-    pad = depth - 5 * rows
-    sx_hi, sx_lo = split(sx)
+    pad = depth - 3 * rows
     re_hi, re_lo = split(keep)
-    left = jnp.concatenate(
-        [sx_hi, sx_lo, sx_hi, re_hi, re_lo, jnp.zeros((pad, chans), F32)], axis=0)
+    left = jnp.concatenate([sx, re_hi, re_lo, jnp.zeros((pad, chans), F32)], axis=0)
     r["left"][...] = left.T.astype(BF16)
     for g in range(groups):
-        b_hi, b_lo = split(bc[:, g * STATE:(g + 1) * STATE])
-        zero = jnp.zeros((rows, STATE), F32)
-        full = jnp.ones((rows, STATE), F32)
-        zpad = jnp.zeros((pad, STATE), F32)
+        zero = jnp.zeros((2 * rows + pad, STATE), F32)
+        full = jnp.ones((2 * rows, STATE), F32)
         r["base"][g, :, :STATE] = jnp.concatenate(
-            [b_hi, b_hi, b_lo, zero, zero, zpad], axis=0).astype(BF16)
+            [bc[:, g * STATE:(g + 1) * STATE], zero], axis=0).astype(BF16)
         r["base"][g, :, STATE:] = jnp.concatenate(
-            [zero, zero, zero, full, full, zpad], axis=0).astype(BF16)
+            [zero[:rows], full, zero[:pad]], axis=0).astype(BF16)
     acc = held[p.tp].astype(F32) + pout[0].astype(F32)
     for d in reversed(far_first(nt)):
         outs[d].wait_recv()
@@ -469,22 +469,25 @@
     rowmod = lax.rem(lax.broadcasted_iota(jnp.int32, (depth, 2 * STATE), 0), rows)
 
     def update(low, high):
-        def body(b, _):
-            mask = jnp.where(rowmod == b, 1.0, 0.0).astype(BF16)
-            for g in range(groups):
-                right = r["base"][g] * mask
-                both = dot(r["left"][g * gch:(g + 1) * gch, :], right)
-                old = state[b, g * hg:(g + 1) * hg].reshape(gch, STATE)
-                new = both[:, STATE:] * old + both[:, :STATE]
-                state[b, g * hg:(g + 1) * hg] = new.reshape(hg, HEAD_DIM, STATE)
+        many = 4 if (high - low) % 4 == 0 else 1
+
+        def body(n, _):
+            for j in range(many):
+                b = low + n * many + j
+                mask = jnp.where(rowmod == b, 1.0, 0.0).astype(BF16)
+                for g in range(groups):
+                    right = r["base"][g] * mask
+                    both = dot(r["left"][g * gch:(g + 1) * gch, :], right)
+                    old = state[b, g * hg:(g + 1) * hg].reshape(gch, STATE)
+                    new = both[:, STATE:] * old + both[:, :STATE]
+                    state[b, g * hg:(g + 1) * hg] = new.reshape(hg, HEAD_DIM, STATE)
             return 0
 
-        return lambda: lax.fori_loop(low, high, body, 0)
-
-    cuts = (rows * 3 // 8, rows * 5 // 8)
+        return lambda: lax.fori_loop(0, (high - low) // many, body, 0)
+
+    cuts = [rows * n // 16 for n in (0, 6, 8, 12, 16)]
     last, finish2 = half_step(p, two, r["mixed"], row("g2"), later["local"], later["swap"],
-                              (update(0, cuts[0]), nothing, update(cuts[0], cuts[1]),
-                               update(cuts[1], rows)), 'b_')
+                              tuple(update(cuts[n], cuts[n + 1]) for n in range(4)), 'b_')
     r["out"][...] = last.astype(BF16)
     finish1()
     finish2()
@@ -529,11 +532,11 @@
                down2=second_down.reshape(2, halfc, width),
                wz=wz.reshape(nt, width, -1), wx=wx.reshape(nt, width, -1),
                wb=wb.reshape(nt, width, -1), wr=wr.reshape(nt, width, -1), wo=wo, state=state)
-    depth = -(-5 * rows // 128) * 128
+    depth = -(-3 * rows // 128) * 128
     scratch = dict(
         wcat=vmem((nt, width, 2 * chans + 2 * groups * STATE), BF16),
         wov=vmem(wo.shape, BF16), ml=DMA((6,)),
-        stb=vmem((rows // 2, chans, 2 * STATE), BF16),
+        stb=vmem((rows // 2, groups, 2 * STATE, chans // groups), BF16),
         held=vmem((nt, rows, width), BF16), f_s=DMA((nt,)), f_r=DMA((nt,)),
         gmv=vmem((nt, 1, width), F32),
         pout=vmem((nt, rows, width), BF16), arrived=vmem((nt, rows, width), BF16),

time: 65.4 us -> 62.6 us (0.957)
  Pallas kernels: 64.6 us -> 61.8 us
    pallas_call x1, Pallas kernels: 61.2 us -> 58.4 us  [per_device(): pl.pallas_call(functools.partial(layer_kernel, nk, nt, names, list(small)...]
where the time goes in v3:
time: 62.6 us; the launch traced here: 62.4 us
  Pallas kernels  61.8 us (99%)
  between operations  0.65 us (1%)
    pallas_call x1, Pallas kernels, per_device(): pl.pallas_call(functools.partial(layer_kernel, nk, nt, names, list(small)...  58.4 us
    pallas_call x1, Pallas kernels, per_device(): pl.pallas_call(flush_kernel, out_shape=(jax.ShapeDtypeStruct(residual.sha...  3.39 us

profile of v3, /device:TPU:0, one launch (start us, length us, event | category | flops | bytes accessed | tf_op | source)
XLA Modules:
  0.0 62.4 jit_solution(5328340403269024443)
XLA Ops:
  0.6 58.4 %layer.1 = (bf16[32,512]{1,0:T(8,128)(2,1)S(1)}, f32[32,8,64,128]{3,2,1,0:T(8,128)S(1)}) custom-call(bf16[32,512]{1,0:T(8,128)(2,1)} %refs_0_.1, bf16[512]{0:T(512)(128)(2,1)} %refs_1_.1, bf16[512]{0:T(512)(128)(2,1)} %refs_2_.1, bf16[2048]{0:T(1024)(128)(2,1)} %refs_3_.1, bf16[512]{0:T(512)(128)(2,1)} %refs_4_.1, bf16[8,2048]{1,0:T(8,128)(2,1)} %bitcast.38, ...), custom_call_target="tpu_custom_call" | custom-call | tf_op jit(solution)/shard_map/layer/pallas_call | solution.py:555
  59.0 3.4 %flush.1 = (bf16[32,512]{1,0:T(8,128)(2,1)}, f32[32,8,64,128]{3,2,1,0:T(8,128)}) custom-call(bf16[32,512]{1,0:T(8,128)(2,1)S(1)} %get-tuple-element.4.a, f32[32,8,64,128]{3,2,1,0:T(8,128)S(1)} %get-tuple-element.5.b), custom_call_target="tpu_custom_call" | custom-call | tf_op jit(solution)/shard_map/flush/pallas_call | solution.py:565

commit v4 on v3

--- a/solution.py
+++ b/solution.py
@@ -65,6 +65,9 @@
 
     def x_from(self, e):
         return lax.rem(self.x + self.nx - e, self.nx)
+
+    def device(self, x, other):
+        return 2 * x + (1 - self.core if other else self.core)
 
     def same_core(self, x):
         return {"tp": 2 * x + self.core}
@@ -94,6 +97,7 @@
         part=vmem((nx, chunks, 2, size, halfc), BF16),
         parr=vmem((nx, chunks, 2, size, halfc), BF16),
         mine=vmem((2, nk // nx * rows, halfc), F32),
+        ahead=vmem((2, size, halfc), F32),
         hid=vmem((2, total, halfc), BF16),
         dpart=vmem((total, width), BF16), dparr=vmem((nk, rows, width), BF16),
         ag_s=DMA((nk,)), ag_r=DMA((nk,)), dd_s=DMA((nk,)), dd_r=DMA((nk,)),
@@ -211,10 +215,12 @@
                 c.wait_recv()
         for e in peers:
             to = p.x_to(e)
-            ready(member(to, i))
             at = chunk(to, i)
             for j, w in enumerate((s["wg"], s["wu"])):
-                s["part"][e, i, j] = (dot_t(s["xg"][0, at, :], w[0])
+                s["ahead"][j] = dot_t(s["xg"][0, at, :], w[0])
+            ready(member(to, i))
+            for j, w in enumerate((s["wg"], s["wu"])):
+                s["part"][e, i, j] = (s["ahead"][j]
                                       + dot_t(s["xg"][1, at, :], w[1])).astype(BF16)
             c = remote(s["part"].at[e, i], s["parr"].at[e, i], s["rs_s"].at[e, i],
                        s["rs_r"].at[e, i], p.same_core(to))
@@ -376,11 +382,13 @@
     held = r["held"]
     held[p.tp] = first.astype(BF16)
     copies = {}
-    for d in far_first(nt):
-        c = remote(held.at[p.tp], held.at[p.tp], r["f_s"].at[d], r["f_r"].at[d],
-                   {"tp": p.tp_to(d)})
+    others = [(e, o) for e in far_first(p.nx) for o in range(2)] + [(0, 1)]
+    for e, o in others:
+        n = 2 * e + o
+        c = remote(held.at[p.tp], held.at[p.tp], r["f_s"].at[n], r["f_r"].at[n],
+                   {"tp": p.device(p.x_to(e), o)})
         c.start()
-        copies[d] = c
+        copies[n] = c
     for c in mixload:
         c.wait()
     for name in small[2:]:
@@ -392,10 +400,10 @@
     total = jnp.zeros((rows, 1), F32)
     proj = jnp.zeros((rows, wcat.shape[-1]), F32)
     raw = jnp.zeros((rows, heads), F32)
-    for d in [0] + list(reversed(far_first(nt))):
-        t = p.tp_from(d)
-        if d:
-            copies[d].wait_recv()
+    for e, o in [(0, 0), (0, 1)] + others[:-1]:
+        t = p.device(p.x_from(e), o)
+        if e or o:
+            copies[2 * e + o].wait_recv()
         v = held[t].astype(F32)
         total = total + jnp.sum(v * v, axis=1, keepdims=True)
         scaled = (v * gmv[t]).astype(BF16)
@@ -440,8 +448,9 @@
     gated = (jnp.concatenate(pieces, axis=1) * row("gg")).astype(BF16)
     pout, arrived = r["pout"], r["arrived"]
     outs = {}
-    for d in far_first(nt) + [0]:
-        to = p.tp_to(d)
+    for e, o in others + [(0, 0)]:
+        d = 2 * e + o
+        to = p.device(p.x_to(e), o)
         wo = r["wov"][:, pl.ds(pl.multiple_of(to * width, width), width)]
         pout[d] = dot(gated, wo).astype(BF16)
         if d:
@@ -461,7 +470,7 @@
         r["base"][g, :, STATE:] = jnp.concatenate(
             [zero[:rows], full, zero[:pad]], axis=0).astype(BF16)
     acc = held[p.tp].astype(F32) + pout[0].astype(F32)
-    for d in reversed(far_first(nt)):
+    for d in outs:
         outs[d].wait_recv()
         acc = acc + arrived[d].astype(F32)
     r["mixed"][...] = acc.astype(BF16)
@@ -485,7 +494,7 @@
 
         return lambda: lax.fori_loop(0, (high - low) // many, body, 0)
 
-    cuts = [rows * n // 16 for n in (0, 6, 8, 12, 16)]
+    cuts = [rows * n // 16 for n in (0, 10, 12, 16, 16)]
     last, finish2 = half_step(p, two, r["mixed"], row("g2"), later["local"], later["swap"],
                               tuple(update(cuts[n], cuts[n + 1]) for n in range(4)), 'b_')
     r["out"][...] = last.astype(BF16)

time: 62.6 us -> 62.7 us (level)
  no operation moved by 1% of the time
where the time goes in v4:
time: 62.7 us; the launch traced here: 62.2 us
  Pallas kernels  61.6 us (98%)
  between operations  0.65 us (1%)
    pallas_call x1, Pallas kernels, per_device(): pl.pallas_call(functools.partial(layer_kernel, nk, nt, names, list(small)...  58.2 us
    pallas_call x1, Pallas kernels, per_device(): pl.pallas_call(flush_kernel, out_shape=(jax.ShapeDtypeStruct(residual.sha...  3.39 us

profile of v4, /device:TPU:0, one launch (start us, length us, event | category | flops | bytes accessed | tf_op | source)
XLA Modules:
  0.0 62.2 jit_solution(11308833453855018336)
XLA Ops:
  0.6 58.2 %layer.1 = (bf16[32,512]{1,0:T(8,128)(2,1)S(1)}, f32[32,8,64,128]{3,2,1,0:T(8,128)S(1)}) custom-call(bf16[32,512]{1,0:T(8,128)(2,1)} %refs_0_.1, bf16[512]{0:T(512)(128)(2,1)} %refs_1_.1, bf16[512]{0:T(512)(128)(2,1)} %refs_2_.1, bf16[2048]{0:T(1024)(128)(2,1)} %refs_3_.1, bf16[512]{0:T(512)(128)(2,1)} %refs_4_.1, bf16[8,2048]{1,0:T(8,128)(2,1)} %bitcast.38, ...), custom_call_target="tpu_custom_call" | custom-call | tf_op jit(solution)/shard_map/layer/pallas_call | solution.py:564
  58.8 3.4 %flush.1 = (bf16[32,512]{1,0:T(8,128)(2,1)}, f32[32,8,64,128]{3,2,1,0:T(8,128)}) custom-call(bf16[32,512]{1,0:T(8,128)(2,1)S(1)} %get-tuple-element.4.a, f32[32,8,64,128]{3,2,1,0:T(8,128)S(1)} %get-tuple-element.5.b), custom_call_target="tpu_custom_call" | custom-call | tf_op jit(solution)/shard_map/flush/pallas_call | solution.py:574
